TPU v7x, 128 devices: a 2x2x16 block of a 8x8x16 slice. The times are simulated.
128 devices in a mesh: grp: 4 (over y, x), ep: 32 (over z, core).
Axes of the slice: x: 2, y: 2, z: 16, core: 2. Of those that a mesh axis runs over, the one named last changes fastest.
The devices are a block of a 8x8x16 slice.
Arguments:
- residual: bfloat16 [64, 4096], P('grp', 'ep'), parts along dimension 0, may hold values from -6 to 6
- head_states: float32 [256, 512, 1024], P(('grp', 'ep')), parts along dimension 0, may hold values from -6 to 6
- first_gain: bfloat16 [4096], replicated, may hold values from 0.099609375 to 1.8984375
- w_query: bfloat16 [4096, 2048], P(None, 'ep'), may hold values from -0.09375 to 0.09375
- w_key: bfloat16 [4096, 2048], P(None, 'ep'), may hold values from -0.09375 to 0.09375
- w_value: bfloat16 [4096, 4096], P(None, 'ep'), may hold values from -0.09375 to 0.09375
- w_gate: bfloat16 [4096, 4096], P(None, 'ep'), may hold values from -0.09375 to 0.09375
- w_low: bfloat16 [4096, 16], replicated, may hold values from -0.09375 to 0.09375
- w_decay: bfloat16 [16, 2048], replicated, may hold values from -15 to 15
- decay_bias: float32 [2048], replicated, may hold values from -40 to 4
- head_gain: bfloat16 [1024], replicated, may hold values from 0.099609375 to 1.8984375
- w_output: bfloat16 [4096, 4096], P(None, 'ep'), may hold values from -0.09375 to 0.09375
- second_gain: bfloat16 [4096], replicated, may hold values from 0.099609375 to 1.8984375
- routes: int32 [64, 2], P('grp'), parts along dimension 0, may hold values from 0 to 31, as said below
- group_logits: float32 [64, 4], P('grp'), parts along dimension 0, may hold values from -12 to 12
- expert_logits: float32 [64, 2], P('grp'), parts along dimension 0, may hold values from -9 to 9
- expert_gate: bfloat16 [32, 4096, 512], P('ep'), may hold values from -0.09375 to 0.09375
- expert_up: bfloat16 [32, 4096, 512], P('ep'), may hold values from -0.09375 to 0.09375
- expert_down: bfloat16 [32, 512, 4096], P('ep'), may hold values from -0.25 to 0.25
Outputs:
- layer_out: bfloat16 [64, 4096], P('grp', 'ep'), parts along dimension 0
- new_states: float32 [256, 512, 1024], P(('grp', 'ep')), parts along dimension 0
There are 4 independent parts, one for each index of `grp`. A program takes and returns all parts, laid end to end along the dimension named above; an argument that names none is the same for every part. Nothing has to cross between parts.
Inputs may be any that keep to these rules, and one draw needn't show every extreme that they name: `routes`: each row names 2 different experts of one group (numbers g * 8 to g * 8 + 7). No expert is named by more than 2 rows, and in every draw all experts of one group are named by exactly 2 rows.
All inputs are finite; a program needn't handle non-finite values.
Results may differ from a plain program's by a relative error of at most 0.014.
Values may be sent and summed in bfloat16 or wider, within the bound.
A program may use at most 128 MiB of HBM per device.

v0:
```python
import jax
import jax.numpy as jnp
import numpy as np
from jax import lax
from jax.sharding import PartitionSpec as P

HEADS = 4
DK = 512
DV = 1024
GROUPS = 4
TOP = 2


norm_eps = 1e-06
decay_tau = 16.0


def from_everyone(shard, axis):
    copies = jnp.broadcast_to(shard, (lax.axis_size(axis), *shard.shape))
    return lax.all_to_all(copies, axis, split_axis=0, concat_axis=0, tiled=True)


def laid_out(tiles, dim):
    dims = list(tiles.shape[1:])
    dims[dim] *= tiles.shape[0]
    return jnp.moveaxis(tiles, 0, dim).reshape(dims)


def collect(shard, axis, dim):
    tiles = from_everyone(shard, axis)
    return laid_out(tiles, dim)


def side_by_side(arrays, axis, split_dim, concat_dim, along):
    ends, at = ([], 0)
    for a in arrays[:-1]:
        at += a.shape[along]
        ends.append(at)
    both = jnp.concatenate(arrays, axis=along)
    return tuple(
        jnp.split(
            lax.all_to_all(both, axis, split_axis=split_dim, concat_axis=concat_dim, tiled=True),
            ends,
            axis=along,
        )
    )


def rms_scale(values, gain):
    floats = values.astype(jnp.float32)
    return (
        floats
        * lax.rsqrt(jnp.mean(floats * floats, axis=-1, keepdims=True) + norm_eps)
        * gain.astype(jnp.float32)
    )


def route_weights(routes, group_logits, expert_logits, per_group):
    group_exp = jnp.exp(group_logits)
    group_prob = group_exp / jnp.sum(group_exp, axis=1, keepdims=True)
    chosen = routes[:, 0] // per_group
    groups_row = jnp.arange(group_logits.shape[1], dtype=jnp.int32)
    picked = jnp.sum(
        group_prob * (chosen[:, None] == groups_row[None, :]).astype(jnp.float32), axis=1
    )
    expert_exp = jnp.exp(expert_logits)
    return expert_exp / jnp.sum(expert_exp, axis=1, keepdims=True) * picked[:, None]


def per_device(
    residual,
    head_states,
    first_gain,
    w_query,
    w_key,
    w_value,
    w_gate,
    w_low,
    w_decay,
    decay_bias,
    head_gain,
    w_output,
    second_gain,
    routes,
    group_logits,
    expert_logits,
    expert_gate,
    expert_up,
    expert_down,
):
    devices = lax.axis_size("ep")
    my_index = lax.axis_index("ep")
    seq_count = residual.shape[0]
    pairs_dev = head_states.shape[0]
    slot_count = max(1, pairs_dev // HEADS)
    rows = collect(residual, "ep", 1)
    normed = rms_scale(rows, first_gain).astype(jnp.bfloat16)
    my_head = my_index * HEADS // devices
    target = jnp.arange(devices, dtype=jnp.int32)[:, None]
    turn = jnp.arange(slot_count, dtype=jnp.int32)[None, :]
    within = jnp.mod(my_head - target * pairs_dev, HEADS) + turn * HEADS
    target_seq = (target * pairs_dev + within) // HEADS
    seq_row = jnp.arange(seq_count, dtype=jnp.int32)[None, None, :]
    picker = (target_seq[:, :, None] == seq_row) & (within < pairs_dev)[:, :, None]
    picker = picker.astype(jnp.bfloat16).reshape(devices * slot_count, seq_count)

    def outgoing(weight):
        projected = jnp.dot(normed, weight, preferred_element_type=jnp.float32).astype(jnp.bfloat16)
        placed = jnp.dot(picker, projected, preferred_element_type=jnp.float32).astype(jnp.bfloat16)
        return placed.reshape(devices, slot_count, projected.shape[1])

    send_query = outgoing(w_query)
    send_key = outgoing(w_key)
    send_value = outgoing(w_value)
    send_gate = outgoing(w_gate)
    incoming = side_by_side((send_query, send_key, send_value, send_gate), "ep", 0, 0, 2)
    pair_ids = my_index * pairs_dev + jnp.arange(pairs_dev, dtype=jnp.int32)
    head_pick = (
        jnp.mod(pair_ids, HEADS)[:, None] == jnp.arange(HEADS, dtype=jnp.int32)[None, :]
    ).astype(jnp.bfloat16)
    turns = np.arange(pairs_dev) // HEADS
    pair_rows = np.arange(pairs_dev)

    def arrange(received):
        merged = jnp.dot(head_pick, received.reshape(HEADS, -1), preferred_element_type=jnp.float32)
        merged = merged.reshape(pairs_dev, devices // HEADS, slot_count, received.shape[2])
        return merged[pair_rows, :, turns, :].reshape(pairs_dev, -1).astype(jnp.bfloat16)

    query = arrange(incoming[0])
    key = arrange(incoming[1])
    value = arrange(incoming[2])
    gate = arrange(incoming[3])
    low = jnp.dot(normed, w_low, preferred_element_type=jnp.float32)
    decay_pre = jnp.dot(low, w_decay.astype(jnp.float32)) + decay_bias
    decay_pre = lax.dynamic_slice_in_dim(
        decay_pre.reshape(seq_count * HEADS, DK), my_index * pairs_dev, pairs_dev, 0
    )
    log_decay = jax.nn.log_sigmoid(decay_pre) / decay_tau
    new_states = (
        head_states * jnp.exp(log_decay)[:, :, None]
        + key.astype(jnp.float32)[:, :, None] * value.astype(jnp.float32)[:, None, :]
    )
    read = jnp.einsum("pk,pkv->pv", query.astype(jnp.float32) * DK ** (-0.5), new_states)
    mixed = (rms_scale(read, head_gain) * jax.nn.silu(gate.astype(jnp.float32))).astype(
        jnp.bfloat16
    )
    gathered = collect(mixed, "ep", 0).reshape(seq_count, HEADS * DV)
    branch = jnp.dot(gathered, w_output, preferred_element_type=jnp.float32).astype(jnp.bfloat16)
    stream = (residual.astype(jnp.float32) + branch.astype(jnp.float32)).astype(jnp.bfloat16)
    whole = collect(stream, "ep", 1)
    expert_in = rms_scale(whole, second_gain).astype(jnp.bfloat16)
    capacity = 2 * seq_count * TOP // devices
    weights = route_weights(routes, group_logits, expert_logits, devices // GROUPS)
    hits = (routes == my_index).astype(jnp.int32)
    mine = jnp.sum(weights * hits.astype(jnp.float32), axis=1)
    routed = jnp.sum(hits, axis=1)
    slot = jnp.cumsum(routed) - routed
    chooser = (slot[None, :] == jnp.arange(capacity, dtype=jnp.int32)[:, None]) & (
        routed[None, :] > 0
    )
    picked = jnp.dot(
        chooser.astype(jnp.bfloat16), expert_in, preferred_element_type=jnp.float32
    ).astype(jnp.bfloat16)
    row_weight = jnp.dot(chooser.astype(jnp.float32), mine)
    gate_part = jnp.dot(picked, expert_gate[0], preferred_element_type=jnp.float32)
    up_part = jnp.dot(picked, expert_up[0], preferred_element_type=jnp.float32)
    active = (jax.nn.silu(gate_part) * up_part * row_weight[:, None]).astype(jnp.bfloat16)
    expert_rows = jnp.dot(active, expert_down[0], preferred_element_type=jnp.float32).astype(
        jnp.bfloat16
    )
    arrived = lax.all_to_all(expert_rows, "ep", split_axis=1, concat_axis=0, tiled=True)
    every = jnp.arange(devices, dtype=jnp.int32)
    hit_all = jnp.sum((routes[:, :, None] == every[None, None, :]).astype(jnp.int32), axis=1)
    slot_all = jnp.cumsum(hit_all, axis=0) - hit_all
    placer = (slot_all[:, :, None] == jnp.arange(capacity, dtype=jnp.int32)[None, None, :]) & (
        hit_all[:, :, None] > 0
    )
    placer = placer.astype(jnp.bfloat16).reshape(seq_count, devices * capacity)
    returned = jnp.dot(placer, arrived, preferred_element_type=jnp.float32)
    layer_out = (stream.astype(jnp.float32) + returned).astype(jnp.bfloat16)
    return (layer_out, new_states)


def solution(mesh):
    return jax.shard_map(
        per_device,
        mesh=mesh,
        in_specs=(
            P("grp", "ep"),
            P(("grp", "ep"), None, None),
            P(),
            P(None, "ep"),
            P(None, "ep"),
            P(None, "ep"),
            P(None, "ep"),
            P(),
            P(),
            P(),
            P(),
            P(None, "ep"),
            P(),
            P("grp", None),
            P("grp", None),
            P("grp", None),
            P("ep", None, None),
            P("ep", None, None),
            P("ep", None, None),
        ),
        out_specs=(P("grp", "ep"), P(("grp", "ep"), None, None)),
        check_vma=False,
    )
```

profile of v0, /device:TPU:69, one launch (start us, length us, event | category | flops | bytes accessed | tf_op | source)
XLA Modules:
  0.0 140.3 jit_solution(9333874315318815657)
XLA Ops:
  0.7 1.5 %broadcast_in_dim.22 = bf16[32,16,128]{2,1,0:T(8,128)(2,1)} broadcast(bf16[16,128]{1,0:T(8,128)(2,1)} %param.29), dimensions={1,2} | broadcast | bytes 135168 | tf_op jit(solution)/shard_map/broadcast_in_dim | solution.py:19
  2.1 18.5 %all-to-all-start = ((bf16[32,16,128]{2,1,0:T(8,128)(2,1)}), bf16[32,16,128]{2,1,0:T(8,128)(2,1)S(1)}, u32[]{:S(2)}, u32[]{:S(2)}) async-start(bf16[32,16,128]{2,1,0:T(8,128)(2,1)} %broadcast_in_dim.22), calls=%async_computation | async-start | bytes 262144 | tf_op jit(solution)/shard_map/all_to_all | solution.py:20
  20.7 0.7 convert_element_type.170
  21.4 0.7 convert_element_type.188
  22.1 0.7 fusion.83
  23.0 0.7 convert_element_type.203
  23.8 12.5 %all-to-all-done = bf16[32,16,128]{2,1,0:T(8,128)(2,1)S(1)} async-done(((bf16[32,16,128]{2,1,0:T(8,128)(2,1)}), bf16[32,16,128]{2,1,0:T(8,128)(2,1)S(1)}, u32[]{:S(2)}, u32[]{:S(2)}) %all-to-all-start) | async-done | bytes 131104 | tf_op jit(solution)/shard_map/all_to_all | solution.py:20
  36.4 1.5 %fusion.8 = bf16[32,1,64]{2,0,1:T(8,128)(2,1)S(1)} fusion(bf16[4096,64]{0,1:T(8,128)(2,1)} %param.32, s32[32]{0:T(128)S(1)} %and_select_fusion.1, pred[32]{0:T(512)(128)(4,1)S(1)} %broadcast_compare_fusion.2, f32[4096]{0:T(1024)S(1)} %convert_element_type.170, f32[16]{0:T(128)S(1)} %add_rsqrt_fusion.2, bf16[32,16,128]{2,1,0:T(8,128)(2,1)S(1)} %all-to-all-done), kind=kOutput, calls=%fused_computation.18 | convolution fusion | flops 8720384 | bytes 676064 | tf_op jit(solution)/shard_map/dot_general | solution.py:109
  37.8 1.5 %fusion.9 = bf16[32,1,64]{2,0,1:T(8,128)(2,1)S(1)} fusion(bf16[4096,64]{0,1:T(8,128)(2,1)} %param.33, s32[32]{0:T(128)S(1)} %and_select_fusion.1, pred[32]{0:T(512)(128)(4,1)S(1)} %broadcast_compare_fusion.2, f32[4096]{0:T(1024)S(1)} %convert_element_type.170, f32[16]{0:T(128)S(1)} %add_rsqrt_fusion.2, bf16[32,16,128]{2,1,0:T(8,128)(2,1)S(1)} %all-to-all-done), kind=kOutput, calls=%fused_computation.19 | convolution fusion | flops 8720384 | bytes 676064 | tf_op jit(solution)/shard_map/dot_general | solution.py:109
  39.7 1.7 %fusion.11 = bf16[32,1,128]{2,0,1:T(8,128)(2,1)S(1)} fusion(bf16[4096,128]{1,0:T(8,128)(2,1)} %param.35, s32[32]{0:T(128)S(1)} %and_select_fusion.1, pred[32]{0:T(512)(128)(4,1)S(1)} %broadcast_compare_fusion.2, f32[4096]{0:T(1024)S(1)} %convert_element_type.170, f32[16]{0:T(128)S(1)} %add_rsqrt_fusion.2, bf16[32,16,128]{2,1,0:T(8,128)(2,1)S(1)} %all-to-all-done), kind=kOutput, calls=%fused_computation.21 | convolution fusion | flops 17177600 | bytes 1204448 | tf_op jit(solution)/shard_map/dot_general | solution.py:109
  41.5 0.5 broadcast.376
  42.0 0.7 reduce.13
  42.7 0.7 reshape.338
  43.4 5.4 %all-to-all-start.1 = ((bf16[32,2,192]{2,1,0:T(2,128)(2,1)}), bf16[32,2,192]{2,1,0:T(2,128)(2,1)S(1)}, u32[]{:S(2)}, u32[]{:S(2)}) async-start(bf16[32,2,192]{2,1,0:T(2,128)(2,1)} %reshape.338), calls=%async_computation.1 | async-start | bytes 65536 | tf_op jit(solution)/shard_map/all_to_all | solution.py:42
  49.3 11.6 %all-to-all-done.1 = bf16[32,2,192]{2,1,0:T(2,128)(2,1)S(1)} async-done(((bf16[32,2,192]{2,1,0:T(2,128)(2,1)}), bf16[32,2,192]{2,1,0:T(2,128)(2,1)S(1)}, u32[]{:S(2)}, u32[]{:S(2)}) %all-to-all-start.1) | async-done | bytes 24608 | tf_op jit(solution)/shard_map/all_to_all | solution.py:42
  61.5 0.6 gather_fusion.2
  62.4 0.6 gather_fusion.1
  63.4 0.6 gather_fusion
  64.1 2.7 %multiply_add_fusion = f32[2,512,1024]{2,1,0:T(8,128)S(1)} fusion(f32[2,512,1024]{2,1,0:T(8,128)} %param.30, f32[2,1024]{1,0:T(2,128)S(1)} %bitcast.187, f32[2,512]{1,0:T(2,128)S(1)} %reshape.297, f32[2,512]{1,0:T(2,128)S(1)} %fusion.70), kind=kLoop, calls=%fused_computation.11 | loop fusion | flops 3145728 | bytes 8404992 | tf_op jit(solution)/shard_map/add | solution.py:140
  66.8 2.0 %copy-done.1 = f32[2,512,1024]{2,1,0:T(8,128)} copy-done((f32[2,512,1024]{2,1,0:T(8,128)}, f32[2,512,1024]{2,1,0:T(8,128)S(1)}, u32[]{:S(2)}) %copy-start.1) | copy-done | bytes 4194328
  69.6 0.6 gather_fusion.3
  70.3 0.7 broadcast_in_dim.31
  71.0 4.8 %all-to-all-start.2 = ((bf16[32,2,1024]{2,1,0:T(2,128)(2,1)}), bf16[32,2,1024]{2,1,0:T(2,128)(2,1)S(1)}, u32[]{:S(2)}, u32[]{:S(2)}) async-start(bf16[32,2,1024]{2,1,0:T(2,128)(2,1)} %broadcast_in_dim.31), calls=%async_computation.2 | async-start | bytes 262144 | tf_op jit(solution)/shard_map/all_to_all | solution.py:20
  75.9 15.8 %all-to-all-done.2 = bf16[32,2,1024]{2,1,0:T(2,128)(2,1)S(1)} async-done(((bf16[32,2,1024]{2,1,0:T(2,128)(2,1)}), bf16[32,2,1024]{2,1,0:T(2,128)(2,1)S(1)}, u32[]{:S(2)}, u32[]{:S(2)}) %all-to-all-start.2) | async-done | bytes 131104 | tf_op jit(solution)/shard_map/all_to_all | solution.py:20
  92.0 0.7 broadcast_in_dim.32
  92.7 5.2 %all-to-all-start.3 = ((bf16[32,16,128]{2,1,0:T(8,128)(2,1)}), bf16[32,16,128]{2,1,0:T(8,128)(2,1)S(1)}, u32[]{:S(2)}, u32[]{:S(2)}) async-start(bf16[32,16,128]{2,1,0:T(8,128)(2,1)} %broadcast_in_dim.32), calls=%async_computation.3 | async-start | bytes 262144 | tf_op jit(solution)/shard_map/all_to_all | solution.py:20
  98.1 15.7 %all-to-all-done.3 = bf16[32,16,128]{2,1,0:T(8,128)(2,1)S(1)} async-done(((bf16[32,16,128]{2,1,0:T(8,128)(2,1)}), bf16[32,16,128]{2,1,0:T(8,128)(2,1)S(1)}, u32[]{:S(2)}, u32[]{:S(2)}) %all-to-all-start.3) | async-done | bytes 131104 | tf_op jit(solution)/shard_map/all_to_all | solution.py:20
  114.2 2.8 %fusion.3 = f32[2,512]{1,0:T(2,128)S(1)} fusion(bf16[2,4096]{1,0:T(2,128)(2,1)S(1)} %convolution_convert_fusion.1, bf16[1,4096,512]{2,1,0:T(8,128)(2,1)} %param.45), kind=kOutput, calls=%fused_computation.9 | convolution fusion | flops 8388608 | bytes 4214784 | tf_op jit(solution)/shard_map/dot_general | solution.py:165
  117.0 5.4 %fusion.5 = bf16[2,32,128]{2,0,1:T(2,128)(2,1)} fusion(bf16[1,512,4096]{2,1,0:T(8,128)(2,1)} %param.47, bf16[2,4096]{1,0:T(2,128)(2,1)S(1)} %convolution_convert_fusion.1, bf16[1,4096,512]{2,1,0:T(8,128)(2,1)} %param.46, f32[2,512]{1,0:T(2,128)S(1)} %fusion.3, f32[2]{0:T(128)S(1)} %convolution_bitcast_fusion.5), kind=kOutput, calls=%fused_computation.13 | convolution fusion | flops 16792576 | bytes 8425480 | tf_op jit(solution)/shard_map/dot_general | solution.py:168
  122.4 5.2 %all-to-all-start.4 = ((bf16[2,32,128]{2,0,1:T(2,128)(2,1)}), bf16[2,32,128]{2,0,1:T(2,128)(2,1)S(1)}, u32[]{:S(2)}, u32[]{:S(2)}) async-start(bf16[2,32,128]{2,0,1:T(2,128)(2,1)} %fusion.5), calls=%async_computation.4 | async-start | bytes 32768 | tf_op jit(solution)/shard_map/all_to_all | solution.py:171
  127.7 11.8 %all-to-all-done.4 = bf16[2,32,128]{2,0,1:T(2,128)(2,1)S(1)} async-done(((bf16[2,32,128]{2,0,1:T(2,128)(2,1)}), bf16[2,32,128]{2,0,1:T(2,128)(2,1)S(1)}, u32[]{:S(2)}, u32[]{:S(2)}) %all-to-all-start.4) | async-done | bytes 16416 | tf_op jit(solution)/shard_map/all_to_all | solution.py:171
  139.5 0.8 fusion.15
  (77 shorter events, 4.9 us)
Async XLA Ops:
  0.6 38.7 %copy-start = (bf16[4096,128]{1,0:T(8,128)(2,1)S(1)}, bf16[4096,128]{1,0:T(8,128)(2,1)}, u32[]{:S(2)}) copy-start(bf16[4096,128]{1,0:T(8,128)(2,1)} %param.34) | copy-start | bytes 3145732
  0.6 48.1 %copy-start.3 = (bf16[4096,16]{0,1:T(8,128)(2,1)S(1)}, bf16[4096,16]{0,1:T(8,128)(2,1)}, u32[]{:S(2)}) copy-start(bf16[4096,16]{0,1:T(8,128)(2,1)} %param.36) | copy-start | bytes 393220
  0.7 48.1 %copy-start.4 = (bf16[16,2048]{1,0:T(8,128)(2,1)S(1)}, bf16[16,2048]{1,0:T(8,128)(2,1)}, u32[]{:S(2)}) copy-start(bf16[16,2048]{1,0:T(8,128)(2,1)} %param.37) | copy-start | bytes 196612
  0.7 48.1 %copy-start.7 = (f32[2048]{0:T(1024)S(1)}, f32[2048]{0:T(1024)}, u32[]{:S(2)}) copy-start(f32[2048]{0:T(1024)} %param.38) | copy-start | bytes 24580
  2.1 34.1 %all-to-all-start = ((bf16[32,16,128]{2,1,0:T(8,128)(2,1)}), bf16[32,16,128]{2,1,0:T(8,128)(2,1)S(1)}, u32[]{:S(2)}, u32[]{:S(2)}) async-start(bf16[32,16,128]{2,1,0:T(8,128)(2,1)} %broadcast_in_dim.22), calls=%async_computation | async-start | bytes 262144 | tf_op jit(solution)/shard_map/all_to_all | solution.py:20
  43.4 17.5 %all-to-all-start.1 = ((bf16[32,2,192]{2,1,0:T(2,128)(2,1)}), bf16[32,2,192]{2,1,0:T(2,128)(2,1)S(1)}, u32[]{:S(2)}, u32[]{:S(2)}) async-start(bf16[32,2,192]{2,1,0:T(2,128)(2,1)} %reshape.338), calls=%async_computation.1 | async-start | bytes 65536 | tf_op jit(solution)/shard_map/all_to_all | solution.py:42
  66.8 2.0 %copy-start.1 = (f32[2,512,1024]{2,1,0:T(8,128)}, f32[2,512,1024]{2,1,0:T(8,128)S(1)}, u32[]{:S(2)}) copy-start(f32[2,512,1024]{2,1,0:T(8,128)S(1)} %multiply_add_fusion) | copy-start | bytes 12582916
  68.9 6.9 %copy-start.9 = (f32[16,2]{0,1:T(2,128)S(1)}, f32[16,2]{0,1:T(2,128)}, u32[]{:S(2)}) copy-start(f32[16,2]{0,1:T(2,128)} %param.44) | copy-start | bytes 388
  68.9 6.9 %copy-start.8 = (f32[16,4]{0,1:T(4,128)S(1)}, f32[16,4]{0,1:T(4,128)}, u32[]{:S(2)}) copy-start(f32[16,4]{0,1:T(4,128)} %param.43) | copy-start | bytes 772
  68.9 7.0 %copy-start.6 = (s32[16,2]{0,1:T(2,128)S(1)}, s32[16,2]{0,1:T(2,128)}, u32[]{:S(2)}) copy-start(s32[16,2]{0,1:T(2,128)} %param.42) | copy-start | bytes 388
  68.9 22.9 %copy-start.2 = (bf16[4096,128]{1,0:T(8,128)(2,1)S(1)}, bf16[4096,128]{1,0:T(8,128)(2,1)}, u32[]{:S(2)}) copy-start(bf16[4096,128]{1,0:T(8,128)(2,1)} %param.40) | copy-start | bytes 3145732
  68.9 22.9 %copy-start.5 = (bf16[16,128]{1,0:T(8,128)(2,1)S(1)}, bf16[16,128]{1,0:T(8,128)(2,1)}, u32[]{:S(2)}) copy-start(bf16[16,128]{1,0:T(8,128)(2,1)} %param.29) | copy-start | bytes 12292
  71.0 20.7 %all-to-all-start.2 = ((bf16[32,2,1024]{2,1,0:T(2,128)(2,1)}), bf16[32,2,1024]{2,1,0:T(2,128)(2,1)S(1)}, u32[]{:S(2)}, u32[]{:S(2)}) async-start(bf16[32,2,1024]{2,1,0:T(2,128)(2,1)} %broadcast_in_dim.31), calls=%async_computation.2 | async-start | bytes 262144 | tf_op jit(solution)/shard_map/all_to_all | solution.py:20
  92.7 21.1 %all-to-all-start.3 = ((bf16[32,16,128]{2,1,0:T(8,128)(2,1)}), bf16[32,16,128]{2,1,0:T(8,128)(2,1)S(1)}, u32[]{:S(2)}, u32[]{:S(2)}) async-start(bf16[32,16,128]{2,1,0:T(8,128)(2,1)} %broadcast_in_dim.32), calls=%async_computation.3 | async-start | bytes 262144 | tf_op jit(solution)/shard_map/all_to_all | solution.py:20
  122.4 17.1 %all-to-all-start.4 = ((bf16[2,32,128]{2,0,1:T(2,128)(2,1)}), bf16[2,32,128]{2,0,1:T(2,128)(2,1)S(1)}, u32[]{:S(2)}, u32[]{:S(2)}) async-start(bf16[2,32,128]{2,0,1:T(2,128)(2,1)} %fusion.5), calls=%async_computation.4 | async-start | bytes 32768 | tf_op jit(solution)/shard_map/all_to_all | solution.py:171
where the time goes:
time: 141 us; the launch traced here: 140 us
  waiting for transfers between devices  67.4 us (48%)
  starting transfers between devices  39.1 us (28%)
  matrix products  16.1 us (11%)
  local copies, waits for them, and re-layouts  9.48 us (7%)
  other arithmetic  7.26 us (5%)
    all_to_all x3, waiting for transfers between devices, from_everyone(): return lax.all_to_all(copies, axis, split_axis=0, concat_axis=0, tiled=True)  43.9 us
    all_to_all x3, starting transfers between devices, from_everyone(): return lax.all_to_all(copies, axis, split_axis=0, concat_axis=0, tiled=True)  28.5 us
    all_to_all x1, waiting for transfers between devices, per_device(): lax.all_to_all(expert_rows, 'ep', split_axis=1, concat_axis=0, tiled=True)  11.8 us
    all_to_all x1, waiting for transfers between devices, side_by_side(): lax.all_to_all(both, axis, split_axis=split_dim, concat_axis=concat_dim,...  11.6 us
    all_to_all x1, starting transfers between devices, side_by_side(): lax.all_to_all(both, axis, split_axis=split_dim, concat_axis=concat_dim,...  5.38 us
    dot_general x1, matrix products, per_device(): jnp.dot(active, expert_down[0], preferred_element_type=jnp.float32)  5.35 us
    all_to_all x1, starting transfers between devices, per_device(): lax.all_to_all(expert_rows, 'ep', split_axis=1, concat_axis=0, tiled=True)  5.22 us
    dot_general x4, matrix products, outgoing(): jnp.dot(picker, projected, preferred_element_type=jnp.float32)  5.01 us
  transfers between devices with their start and end apart: 5, of which 5 were waited for; matrix products, arithmetic and copies ran while one was open for 3% of the time, Pallas kernels for 0%

commit v1 on v0

v1 whole, which is shorter than its diff:
```python
import functools
import jax
import jax.numpy as jnp
from jax import lax
from jax.experimental import pallas as pl
from jax.experimental.pallas import tpu as pltpu
from jax.sharding import PartitionSpec as P

HEADS = 4
GROUPS = 4
TOP = 2
EPS = 1e-6
TAU = 16.0
MESH = pl.DeviceIdType.MESH
BF16 = jnp.bfloat16
F32 = jnp.float32
NT = (((1,), (1,)), ((), ()))
NN = (((1,), (0,)), ((), ()))
TN = (((0,), (0,)), ((), ()))


def mm(a, b, dims=NN, precision=None):
    return lax.dot_general(a, b, dims, precision=precision, preferred_element_type=F32)


def kernel(
    N,
    res_h, st_h, g1_h, wq_h, wk_h, wv_h, wg_h, wl_h, wd_h, bias_h, hg_h, wo_h, g2_h,
    rt_h, gl_h, el_h, eg_h, eu_h, ed_h,
    out_ref, ns_h,
    res, st, g1, wqk, wvg, wd, bias, hg, wo, g2, rt, gl, el, eg, eu, ed,
    g1f, g2f, xb, pj, rq, decb, cols, mx, mb, ff, ch, sb, eb, db, rb, strm,
    lsem, ssem, rsem, r1, r3, r4, osem,
):
    me = lax.axis_index("ep")
    C = N // 2
    z, c = me // 2, lax.rem(me, 2)
    T = res.shape[0]
    far = [C // 2] + [s * d for d in range(C // 2 - 1, 0, -1) for s in (1, -1)]
    near = far[::-1]

    def chip(o):
        return lax.rem(z + (o + C), C)

    barrier = pltpu.get_barrier_semaphore()
    for d in range(1, N):
        pl.semaphore_signal(barrier, inc=1, device_id={"ep": lax.rem(me + d, N)}, device_id_type=MESH)

    half = pl.multiple_of(c * 1024, 1024)
    hrow = pl.multiple_of(c * 8, 8)
    loads = [
        (res_h, res), (g1_h, g1), (g2_h, g2), (hg_h, hg), (rt_h, rt), (gl_h, gl), (el_h, el),
        (bias_h.at[pl.ds(hrow, 8)], bias), (wd_h.at[:, pl.ds(half, 1024)], wd),
        (wq_h, wqk.at[pl.ds(0, 64)]), (wk_h, wqk.at[pl.ds(64, 64)]), (wl_h, wqk.at[pl.ds(128, 16)]),
        (wv_h, wvg.at[:, pl.ds(0, 128)]), (wg_h, wvg.at[:, pl.ds(128, 128)]),
        (st_h, st), (wo_h, wo), (eg_h.at[0], eg), (eu_h.at[0], eu), (ed_h.at[0], ed),
    ]
    cps = [pltpu.make_async_copy(s, d, lsem.at[i]) for i, (s, d) in enumerate(loads)]
    for cp in cps:
        cp.start()
    for cp in cps[:9]:
        cp.wait()

    xb[me] = res[...]
    g1f[...] = g1[...].astype(F32)
    g2f[...] = g2[...].astype(F32)

    routes = rt[...]
    gexp = jnp.exp(gl[...])
    gprob = gexp / jnp.sum(gexp, axis=0, keepdims=True)
    per_group = N // GROUPS
    grow = lax.broadcasted_iota(jnp.int32, gprob.shape, 0)
    lo = grow * per_group
    first = jnp.broadcast_to(routes[0:1], gprob.shape)
    inside = (first >= lo) & (first < lo + per_group)
    gpick = jnp.sum(jnp.where(inside, gprob, 0.0), axis=0, keepdims=True)
    eexp = jnp.exp(el[...])
    weight = eexp / jnp.sum(eexp, axis=0, keepdims=True) * gpick
    before = (
        lax.broadcasted_iota(jnp.int32, (T, T), 0) < lax.broadcasted_iota(jnp.int32, (T, T), 1)
    ).astype(BF16)
    slots_all = 2 * N
    row = lax.broadcasted_iota(jnp.int32, (slots_all, T), 0)
    expert = lax.shift_right_logical(row, 1)
    r0 = jnp.broadcast_to(routes[0:1], (slots_all, T))
    r1_ = jnp.broadcast_to(routes[1:2], (slots_all, T))
    hit = jnp.where((r0 == expert) | (r1_ == expert), 1.0, 0.0)
    slot = mm(hit.astype(BF16), before)
    parity = (row - 2 * expert).astype(F32)
    ch[...] = jnp.where(slot == parity, hit, 0.0)
    my_hit = jnp.where(routes == me, 1.0, 0.0)
    share = jnp.sum(weight * my_hit, axis=0, keepdims=True)
    mine = jnp.sum(my_hit, axis=0, keepdims=True)
    my_slot = mm(jnp.broadcast_to(mine, (8, T)).astype(BF16), before)
    srow = lax.broadcasted_iota(jnp.int32, (8, T), 0).astype(F32)
    rw = jnp.sum(jnp.where(my_slot == srow, jnp.broadcast_to(mine * share, (8, T)), 0.0), axis=1, keepdims=True)

    pl.semaphore_wait(barrier, N - 1)

    def remote(src, dst, send, recv, j):
        return pltpu.make_async_remote_copy(
            src_ref=src, dst_ref=dst, send_sem=send, recv_sem=recv, device_id={"ep": j}, device_id_type=MESH
        )

    def spread(src, buf, stage, sem):
        for o in far:
            for cc in (0, 1):
                remote(src, buf.at[me], ssem.at[stage], sem.at[z], 2 * chip(o) + cc).start()
        remote(src, buf.at[me], ssem.at[stage], sem.at[z], 2 * z + 1 - c).start()

    def arrived(buf, sem, o):
        zz = chip(o)
        ref = buf.at[pl.ds(2 * zz, 2)] if o else buf.at[2 * zz]
        remote(ref, ref, sem.at[zz], sem.at[zz], me).wait_recv()
        return zz

    spread(res, xb, 0, r1)
    for cp in cps[9:14]:
        cp.wait()
    ssq = jnp.zeros((T, 256), F32)
    vg = jnp.zeros((T, 256), F32)
    qk = jnp.zeros((T, 144), F32)
    for o in [0] + near:
        zz = arrived(xb, r1, o)
        x = jnp.concatenate([xb[2 * zz], xb[2 * zz + 1]], axis=1).astype(F32)
        gain = jnp.concatenate([g1f[pl.ds(2 * zz, 1)], g1f[pl.ds(2 * zz + 1, 1)]], axis=1)
        ssq = ssq + x * x
        y = (x * gain).astype(BF16)
        at = pl.multiple_of(zz * 256, 256)
        vg = vg + mm(y, wvg[pl.ds(at, 256), :])
        qk = qk + mm(y, wqk[:, pl.ds(at, 256)], NT)
    scale = lax.rsqrt(jnp.sum(ssq, axis=1, keepdims=True) * (1.0 / (128 * N)) + EPS)
    vg = (vg * scale).astype(BF16).astype(F32)
    low = qk[:, 128:144] * scale
    qk = (qk[:, :128] * scale).astype(BF16).astype(F32)

    for s in range(T):
        pj[s, 0:1] = vg[s : s + 1, :128]
        pj[s, 1:2] = vg[s : s + 1, 128:]
        pj[s, 2:3] = qk[s : s + 1]
    S = N // 2
    core = me // S
    mine_at = lax.rem(me, S)
    for o in far:
        s = chip(o)
        remote(pj.at[s], rq.at[mine_at], ssem.at[1], rsem.at[0], 2 * s + core).start()

    @pl.when(core != c)
    def _():
        remote(pj.at[z], rq.at[mine_at], ssem.at[1], rsem.at[0], 2 * z + core).start()

    @pl.when(core == c)
    def _():
        rq[mine_at] = pj[z]

    pick = jnp.where(lax.broadcasted_iota(jnp.int32, (T, 128), 0) == z, 1.0, 0.0)
    lowcol = mm(low, pick, TN, lax.Precision.HIGHEST)
    pre = mm(wd[...].astype(F32), lowcol, TN, lax.Precision.HIGHEST)
    bcol = bias[...].T
    for b in range(8):
        v = pre[b * 128 : (b + 1) * 128] + bcol[:, b : b + 1]
        ls = jnp.minimum(v, 0.0) - jnp.log(1.0 + jnp.exp(-jnp.abs(v)))
        decb[b * 128 : (b + 1) * 128] = jnp.exp(ls * (1.0 / TAU))
    cps[14].wait()

    @pl.when(core == c)
    def _():
        ref = rq.at[pl.ds(0, S - 1)]
        remote(ref, ref, rsem.at[0], rsem.at[0], me).wait_recv()

    @pl.when(core != c)
    def _():
        remote(rq, rq, rsem.at[0], rsem.at[0], me).wait_recv()

    allv = rq[...]
    val = allv[:, 0, :]
    gat = allv[:, 1, :]
    ct = allv[:, 2, :].T
    cols[:, 0:16] = ct
    prod = ct[0:64] * ct[64:128]
    dotqk = jnp.sum(prod, axis=0, keepdims=True)
    lane = lax.broadcasted_iota(jnp.int32, (1, 16), 1)
    sub8 = lax.broadcasted_iota(jnp.int32, (8, 128), 0)
    mixed = []
    for j in range(2):
        acc = [jnp.zeros((8, 128), F32) for _ in range(8)]
        for i in range(8):
            qd = jnp.broadcast_to(ct[0:64, 8 * j + i : 8 * j + i + 1], (64, 128)) * decb[j * 512 + i * 64 : j * 512 + (i + 1) * 64]
            for k in range(8):
                q8 = qd[8 * k : 8 * k + 8]
                r = i * 64 + 8 * k
                for l in range(8):
                    acc[l] = acc[l] + q8 * st[j, r : r + 8, 128 * l : 128 * l + 128]
        read = jnp.zeros((8, 128), F32)
        for l in range(8):
            read = jnp.where(sub8 == l, jnp.sum(acc[l], axis=0, keepdims=True), read)
        sqk = jnp.sum(jnp.where((lane >= 8 * j) & (lane < 8 * j + 8), dotqk, 0.0), axis=1, keepdims=True)
        read = (read + sqk * val[8 * j : 8 * j + 8]) * (512 ** -0.5)
        tot = jnp.sum(jnp.sum(read * read, axis=1, keepdims=True), axis=0, keepdims=True)
        nrm = lax.rsqrt(tot * (1.0 / 1024) + EPS)
        g = gat[8 * j : 8 * j + 8]
        mixed.append(read * nrm * hg[...].astype(F32) * (g / (1.0 + jnp.exp(-g))))
    mixed = jnp.concatenate(mixed, axis=0).astype(BF16)
    mx[...] = mixed
    mb[me] = mixed
    spread(mx, mb, 2, r3)

    for j in range(2):
        for i in range(8):
            kc = jnp.broadcast_to(ct[64:128, 8 * j + i : 8 * j + i + 1], (64, 128))
            for k in range(8):
                r = i * 64 + 8 * k
                d8 = decb[j * 512 + r : j * 512 + r + 8]
                k8 = kc[8 * k : 8 * k + 8]
                for l in range(8):
                    sl = (j, slice(r, r + 8), slice(128 * l, 128 * l + 128))
                    st[sl] = st[sl] * d8 + k8 * val[8 * j + l : 8 * j + l + 1]
    outcp = pltpu.make_async_copy(st, ns_h, osem.at[0])
    outcp.start()
    cps[15].wait()
    for o in [0] + near:
        arrived(mb, r3, o)
    PITCH = 17
    for s in range(T):
        for cc in range(2):
            base = cc * PITCH * T + s * PITCH
            ff[base : base + 16] = mb[2 * s + cc].astype(F32)
    lhs = []
    for kb in range(N):
        base = (kb // 16) * PITCH * T + kb % 16
        lhs.append(ff[pl.ds(base, T, stride=PITCH), :].astype(BF16))
    branch = mm(jnp.concatenate(lhs, axis=1), wo[...]).astype(BF16).astype(F32)
    stream = (res[...].astype(F32) + branch).astype(BF16)
    strm[...] = stream

    picked = mm(ch[...].astype(BF16), stream)
    sb[...] = picked.reshape(N, 2, 128).astype(sb.dtype)
    for o in far:
        for cc in (0, 1):
            j = 2 * chip(o) + cc
            remote(sb.at[j], eb.at[me], ssem.at[3], r4.at[z], j).start()
    remote(sb.at[2 * z + 1 - c], eb.at[me], ssem.at[3], r4.at[z], 2 * z + 1 - c).start()
    eb[me] = sb[me]
    for cp in cps[16:18]:
        cp.wait()
    ssq = jnp.zeros((2, 256), F32)
    ga = jnp.zeros((2, 512), F32)
    up = jnp.zeros((2, 512), F32)
    for o in [0] + near:
        zz = arrived(eb, r4, o)
        x = jnp.concatenate([eb[2 * zz], eb[2 * zz + 1]], axis=1).astype(F32)
        gain = jnp.concatenate([g2f[pl.ds(2 * zz, 1)], g2f[pl.ds(2 * zz + 1, 1)]], axis=1)
        ssq = ssq + x * x
        y = (x * gain).astype(BF16)
        at = pl.multiple_of(zz * 256, 256)
        ga = ga + mm(y, eg[pl.ds(at, 256), :])
        up = up + mm(y, eu[pl.ds(at, 256), :])
    scale = lax.rsqrt(jnp.sum(ssq, axis=1, keepdims=True) * (1.0 / (128 * N)) + EPS)
    ga = ga * scale
    act = (ga / (1.0 + jnp.exp(-ga)) * (up * scale) * rw[0:2]).astype(BF16)

    cps[18].wait()
    for o in far + [0]:
        zz = chip(o)
        at = pl.multiple_of(zz * 256, 256)
        rows = mm(act, ed[:, pl.ds(at, 256)])
        for cc in (0, 1):
            db[2 * zz + cc] = rows[:, 128 * cc : 128 * cc + 128].astype(BF16).astype(db.dtype)
            if o:
                remote(db.at[2 * zz + cc], rb.at[me], ssem.at[4], rsem.at[1], 2 * zz + cc).start()
    remote(db.at[2 * z + 1 - c], rb.at[me], ssem.at[4], rsem.at[1], 2 * z + 1 - c).start()
    rb[me] = db[me]
    ref = rb.at[pl.ds(0, N - 1)]
    remote(ref, ref, rsem.at[1], rsem.at[1], me).wait_recv()
    back = mm(ch[...].astype(BF16), rb[...].reshape(2 * N, 128).astype(BF16), TN)
    out_ref[...] = (strm[...].astype(F32) + back).astype(BF16)

    for stage, ref in ((0, xb.at[pl.ds(0, N - 1)]), (2, mb.at[pl.ds(0, N - 1)]), (3, eb.at[pl.ds(0, N - 1)]), (4, rb.at[pl.ds(0, N - 1)])):
        remote(ref, ref, ssem.at[stage], ssem.at[stage], me).wait_send()

    @pl.when(core == c)
    def _():
        ref = rq.at[pl.ds(0, S - 1)]
        remote(ref, ref, ssem.at[1], ssem.at[1], me).wait_send()

    @pl.when(core != c)
    def _():
        remote(rq, rq, ssem.at[1], ssem.at[1], me).wait_send()

    outcp.wait()


def per_device(N, residual, head_states, first_gain, w_query, w_key, w_value, w_gate, w_low, w_decay, decay_bias,
               head_gain, w_output, second_gain, routes, group_logits, expert_logits, expert_gate, expert_up, expert_down):
    args = (
        residual, head_states, first_gain.reshape(-1, 128), w_query.T, w_key.T, w_value, w_gate, w_low.T, w_decay,
        decay_bias.reshape(-1, 128), head_gain.reshape(-1, 128), w_output, second_gain.reshape(-1, 128),
        routes.T, group_logits.T, expert_logits.T, expert_gate, expert_up, expert_down,
    )
    V = pltpu.VMEM
    D = 128 * N
    SB = BF16
    scratch = [
        V((16, 128), BF16), V((2, 512, 1024), F32), V((N, 128), BF16), V((144, D), BF16), V((D, 256), BF16),
        V((16, 1024), BF16), V((8, 128), F32), V((8, 128), BF16), V((D, 128), BF16), V((N, 128), BF16),
        V((2, 16), jnp.int32), V((4, 16), F32), V((2, 16), F32), V((D, 512), BF16), V((D, 512), BF16), V((512, D), BF16),
        V((N, 128), F32), V((N, 128), F32), V((N, 16, 128), BF16), V((16, 4, 128), F32), V((16, 4, 128), F32),
        V((1024, 128), F32), V((128, 128), F32), V((16, 128), BF16), V((N, 16, 128), BF16), V((2 * 17 * 16, 128), F32),
        V((2 * N, 16), F32), V((N, 2, 128), SB), V((N, 2, 128), SB), V((N, 2, 128), SB), V((N, 2, 128), SB), V((16, 128), BF16),
        pltpu.SemaphoreType.DMA((19,)), pltpu.SemaphoreType.DMA((5,)), pltpu.SemaphoreType.DMA((2,)),
        pltpu.SemaphoreType.DMA((N // 2,)), pltpu.SemaphoreType.DMA((N // 2,)), pltpu.SemaphoreType.DMA((N // 2,)),
        pltpu.SemaphoreType.DMA((1,)),
    ]
    return pl.pallas_call(
        functools.partial(kernel, N),
        out_shape=(jax.ShapeDtypeStruct(residual.shape, BF16), jax.ShapeDtypeStruct(head_states.shape, F32)),
        in_specs=[pl.BlockSpec(memory_space=pl.ANY)] * len(args),
        out_specs=(pl.BlockSpec(memory_space=pltpu.VMEM), pl.BlockSpec(memory_space=pl.ANY)),
        scratch_shapes=scratch,
        compiler_params=pltpu.CompilerParams(collective_id=0, has_side_effects=True, vmem_limit_bytes=56 * 1024 * 1024),
    )(*args)


def solution(mesh):
    N = mesh.shape["ep"]
    return jax.shard_map(
        functools.partial(per_device, N),
        mesh=mesh,
        in_specs=(
            P("grp", "ep"), P(("grp", "ep"), None, None), P(), P(None, "ep"), P(None, "ep"), P(None, "ep"), P(None, "ep"),
            P(), P(), P(), P(), P(None, "ep"), P(), P("grp", None), P("grp", None), P("grp", None),
            P("ep", None, None), P("ep", None, None), P("ep", None, None),
        ),
        out_specs=(P("grp", "ep"), P(("grp", "ep"), None, None)),
        check_vma=False,
    )
```

time: 141 us -> 65.1 us (0.46)
  waiting for transfers between devices: 67.4 us -> 0 us
  Pallas kernels: 0 us -> 58.2 us
  starting transfers between devices: 39.1 us -> 0 us
  matrix products: 16.1 us -> 0 us
  other arithmetic: 7.26 us -> 0 us
  local copies, waits for them, and re-layouts: 9.48 us -> 6.05 us
    all_to_all x5 -> x0, waiting for transfers between devices: 67.4 us -> none  [the longest x3 43.9 us: from_everyone(): return lax.all_to_all(copies, axis, split_axis=0, concat_axis=0, tiled=True)]
    pallas_call x0 -> x1, Pallas kernels: none -> 58.2 us  [per_device(): pl.pallas_call(functools.partial(kernel, N), out_shape=(jax.ShapeDtypeStr...]
    all_to_all x5 -> x0, starting transfers between devices: 39.1 us -> none  [the longest x3 28.5 us: from_everyone(): return lax.all_to_all(copies, axis, split_axis=0, concat_axis=0, tiled=True)]
    dot_general x16 -> x0, matrix products: 16.1 us -> none  [the longest x1 5.35 us: per_device(): jnp.dot(active, expert_down[0], preferred_element_type=jnp.float32)]
    unnamed x23 -> x2, local copies, waits for them, and re-layouts: 2.87 us -> 6.05 us
    broadcast_in_dim x3 -> x0, local copies, waits for them, and re-layouts: 2.84 us -> none  [from_everyone(): copies = jnp.broadcast_to(shard, (lax.axis_size(axis), *shard.shape))]
    add x1 -> x0, other arithmetic: 2.73 us -> none  [per_device(): head_states * jnp.exp(log_decay)[:, :, None]]
    gather x4 -> x0, local copies, waits for them, and re-layouts: 2.25 us -> none  [arrange(): merged[pair_rows, :, turns, :].reshape(pairs_dev, -1).astype(jnp.bfloat16)]
  transfers between devices with their start and end apart: 5 -> 0, of which waited for: 5 -> 0; matrix products, arithmetic and copies ran while one was open for 3% -> 0% of each run, Pallas kernels for 0% -> 0%
where the time goes in v1:
time: 65.1 us; the launch traced here: 64.9 us
  Pallas kernels  58.2 us (89%)
  local copies, waits for them, and re-layouts  6.05 us (9%)
    pallas_call x1, Pallas kernels, per_device(): pl.pallas_call(functools.partial(kernel, N), out_shape=(jax.ShapeDtypeStr...  58.2 us
    unnamed x2, local copies, waits for them, and re-layouts  6.05 us

profile of v1, /device:TPU:69, one launch (start us, length us, event | category | flops | bytes accessed | tf_op | source)
XLA Modules:
  0.0 64.9 jit_solution(2286795122438187526)
XLA Ops:
  0.6 58.2 %shard_map.194 = (bf16[16,128]{1,0:T(8,128)(2,1)}, f32[2,512,1024]{2,1,0:T(8,128)}) custom-call(bf16[16,128]{1,0:T(8,128)(2,1)} %res_h.1, f32[2,512,1024]{2,1,0:T(8,128)} %st_h.1, bf16[32,128]{1,0:T(8,128)(2,1)} %bitcast.13, bf16[64,4096]{1,0:T(8,128)(2,1)} %bitcast.10, bf16[64,4096]{1,0:T(8,128)(2,1)} %bitcast.11, bf16[4096,128]{1,0:T(8,128)(2,1)} %wv_h.1, ...), custom_call_target="tpu_custom_call" | custom-call | tf_op jit(solution)/shard_map/pallas_call | solution.py:314
  58.9 1.3 %copy.23 = bf16[16,128]{1,0:T(8,128)(2,1)} copy(bf16[16,128]{1,0:T(8,128)(2,1)} %get-tuple-element.4) | data formatting | bytes 8192
  60.1 4.8 %copy.24 = f32[2,512,1024]{2,1,0:T(8,128)} copy(f32[2,512,1024]{2,1,0:T(8,128)} %get-tuple-element.5) | data formatting | bytes 8388608

commit v2 on v1

--- a/solution.py
+++ b/solution.py
@@ -27,8 +27,8 @@
     N,
     res_h, st_h, g1_h, wq_h, wk_h, wv_h, wg_h, wl_h, wd_h, bias_h, hg_h, wo_h, g2_h,
     rt_h, gl_h, el_h, eg_h, eu_h, ed_h,
-    out_ref, ns_h,
-    res, st, g1, wqk, wvg, wd, bias, hg, wo, g2, rt, gl, el, eg, eu, ed,
+    out_ref, st,
+    res, g1, wqk, wvg, wd, bias, hg, wo, g2, rt, gl, el, eg, eu, ed,
     g1f, g2f, xb, pj, rq, decb, cols, mx, mb, ff, ch, sb, eb, db, rb, strm,
     lsem, ssem, rsem, r1, r3, r4, osem,
 ):
@@ -43,8 +43,12 @@
         return lax.rem(z + (o + C), C)
 
     barrier = pltpu.get_barrier_semaphore()
-    for d in range(1, N):
-        pl.semaphore_signal(barrier, inc=1, device_id={"ep": lax.rem(me + d, N)}, device_id_type=MESH)
+    reach = C // 4
+    close = [o for o in near if abs(o) <= reach]
+    for o in close:
+        for cc in (0, 1):
+            pl.semaphore_signal(barrier, inc=1, device_id={"ep": 2 * chip(o) + cc}, device_id_type=MESH)
+    pl.semaphore_signal(barrier, inc=1, device_id={"ep": 2 * z + 1 - c}, device_id_type=MESH)
 
     half = pl.multiple_of(c * 1024, 1024)
     hrow = pl.multiple_of(c * 8, 8)
@@ -56,7 +60,7 @@
         (st_h, st), (wo_h, wo), (eg_h.at[0], eg), (eu_h.at[0], eu), (ed_h.at[0], ed),
     ]
     cps = [pltpu.make_async_copy(s, d, lsem.at[i]) for i, (s, d) in enumerate(loads)]
-    for cp in cps:
+    for cp in cps[:14]:
         cp.start()
     for cp in cps[:9]:
         cp.wait()
@@ -95,18 +99,13 @@
     srow = lax.broadcasted_iota(jnp.int32, (8, T), 0).astype(F32)
     rw = jnp.sum(jnp.where(my_slot == srow, jnp.broadcast_to(mine * share, (8, T)), 0.0), axis=1, keepdims=True)
 
-    pl.semaphore_wait(barrier, N - 1)
+    pl.semaphore_wait(barrier, 2 * len(close) + 1)
 
     def remote(src, dst, send, recv, j):
         return pltpu.make_async_remote_copy(
             src_ref=src, dst_ref=dst, send_sem=send, recv_sem=recv, device_id={"ep": j}, device_id_type=MESH
         )
 
-    def spread(src, buf, stage, sem):
-        for o in far:
-            for cc in (0, 1):
-                remote(src, buf.at[me], ssem.at[stage], sem.at[z], 2 * chip(o) + cc).start()
-        remote(src, buf.at[me], ssem.at[stage], sem.at[z], 2 * z + 1 - c).start()
 
     def arrived(buf, sem, o):
         zz = chip(o)
@@ -114,14 +113,26 @@
         remote(ref, ref, sem.at[zz], sem.at[zz], me).wait_recv()
         return zz
 
-    spread(res, xb, 0, r1)
+    for o in close[::-1]:
+        for cc in (0, 1):
+            remote(res, xb.at[me], ssem.at[0], r1.at[z], 2 * chip(o) + cc).start()
+    remote(res, xb.at[me], ssem.at[0], r1.at[z], 2 * z + 1 - c).start()
+    for o in close + [0]:
+        zz = arrived(xb, r1, o)
+        if 0 < o <= reach or -reach < o < 0:
+            to = chip(-reach if o > 0 else reach)
+            for cc in (0, 1):
+                blk = xb.at[2 * zz + c]
+                remote(blk, blk, ssem.at[0], r1.at[zz], 2 * to + cc).start()
+    for cp in cps[14:]:
+        cp.start()
     for cp in cps[9:14]:
         cp.wait()
     ssq = jnp.zeros((T, 256), F32)
     vg = jnp.zeros((T, 256), F32)
     qk = jnp.zeros((T, 144), F32)
     for o in [0] + near:
-        zz = arrived(xb, r1, o)
+        zz = chip(o) if abs(o) <= reach else arrived(xb, r1, o)
         x = jnp.concatenate([xb[2 * zz], xb[2 * zz + 1]], axis=1).astype(F32)
         gain = jnp.concatenate([g1f[pl.ds(2 * zz, 1)], g1f[pl.ds(2 * zz + 1, 1)]], axis=1)
         ssq = ssq + x * x
@@ -203,7 +214,9 @@
     mixed = jnp.concatenate(mixed, axis=0).astype(BF16)
     mx[...] = mixed
     mb[me] = mixed
-    spread(mx, mb, 2, r3)
+    for o in far:
+        remote(mx, mb.at[me], ssem.at[2], r3.at[z], 2 * chip(o) + c).start()
+    remote(mx, mb.at[me], ssem.at[2], rsem.at[2], 2 * z + 1 - c).start()
 
     for j in range(2):
         for i in range(8):
@@ -215,20 +228,22 @@
                 for l in range(8):
                     sl = (j, slice(r, r + 8), slice(128 * l, 128 * l + 128))
                     st[sl] = st[sl] * d8 + k8 * val[8 * j + l : 8 * j + l + 1]
-    outcp = pltpu.make_async_copy(st, ns_h, osem.at[0])
-    outcp.start()
     cps[15].wait()
-    for o in [0] + near:
-        arrived(mb, r3, o)
+    for o in near:
+        zz = chip(o)
+        blk = mb.at[2 * zz + c]
+        remote(blk, blk, r3.at[zz], r3.at[zz], me).wait_recv()
+        remote(blk, blk, ssem.at[2], rsem.at[2], 2 * z + 1 - c).start()
     PITCH = 17
     for s in range(T):
-        for cc in range(2):
-            base = cc * PITCH * T + s * PITCH
-            ff[base : base + 16] = mb[2 * s + cc].astype(F32)
+        ff[c, s * PITCH : s * PITCH + 16] = mb[2 * s + c].astype(F32)
+    half_mb = mb.at[pl.ds(0, C)]
+    remote(half_mb, half_mb, rsem.at[2], rsem.at[2], me).wait_recv()
+    for s in range(T):
+        ff[1 - c, s * PITCH : s * PITCH + 16] = mb[2 * s + 1 - c].astype(F32)
     lhs = []
     for kb in range(N):
-        base = (kb // 16) * PITCH * T + kb % 16
-        lhs.append(ff[pl.ds(base, T, stride=PITCH), :].astype(BF16))
+        lhs.append(ff[kb // 16, pl.ds(kb % 16, T, stride=PITCH), :].astype(BF16))
     branch = mm(jnp.concatenate(lhs, axis=1), wo[...]).astype(BF16).astype(F32)
     stream = (res[...].astype(F32) + branch).astype(BF16)
     strm[...] = stream
@@ -287,8 +302,6 @@
     def _():
         remote(rq, rq, ssem.at[1], ssem.at[1], me).wait_send()
 
-    outcp.wait()
-
 
 def per_device(N, residual, head_states, first_gain, w_query, w_key, w_value, w_gate, w_low, w_decay, decay_bias,
                head_gain, w_output, second_gain, routes, group_logits, expert_logits, expert_gate, expert_up, expert_down):
@@ -298,27 +311,47 @@
         routes.T, group_logits.T, expert_logits.T, expert_gate, expert_up, expert_down,
     )
     V = pltpu.VMEM
+    args = tuple(pltpu.with_memory_space_constraint(a, pltpu.HBM) for a in args)
     D = 128 * N
     SB = BF16
     scratch = [
-        V((16, 128), BF16), V((2, 512, 1024), F32), V((N, 128), BF16), V((144, D), BF16), V((D, 256), BF16),
+        V((16, 128), BF16), V((N, 128), BF16), V((144, D), BF16), V((D, 256), BF16),
         V((16, 1024), BF16), V((8, 128), F32), V((8, 128), BF16), V((D, 128), BF16), V((N, 128), BF16),
         V((2, 16), jnp.int32), V((4, 16), F32), V((2, 16), F32), V((D, 512), BF16), V((D, 512), BF16), V((512, D), BF16),
         V((N, 128), F32), V((N, 128), F32), V((N, 16, 128), BF16), V((16, 4, 128), F32), V((16, 4, 128), F32),
-        V((1024, 128), F32), V((128, 128), F32), V((16, 128), BF16), V((N, 16, 128), BF16), V((2 * 17 * 16, 128), F32),
+        V((1024, 128), F32), V((128, 128), F32), V((16, 128), BF16), V((N, 16, 128), BF16), V((2, 17 * 16, 128), F32),
         V((2 * N, 16), F32), V((N, 2, 128), SB), V((N, 2, 128), SB), V((N, 2, 128), SB), V((N, 2, 128), SB), V((16, 128), BF16),
-        pltpu.SemaphoreType.DMA((19,)), pltpu.SemaphoreType.DMA((5,)), pltpu.SemaphoreType.DMA((2,)),
+        pltpu.SemaphoreType.DMA((19,)), pltpu.SemaphoreType.DMA((5,)), pltpu.SemaphoreType.DMA((3,)),
         pltpu.SemaphoreType.DMA((N // 2,)), pltpu.SemaphoreType.DMA((N // 2,)), pltpu.SemaphoreType.DMA((N // 2,)),
         pltpu.SemaphoreType.DMA((1,)),
     ]
-    return pl.pallas_call(
+    lo, ns = pl.pallas_call(
         functools.partial(kernel, N),
         out_shape=(jax.ShapeDtypeStruct(residual.shape, BF16), jax.ShapeDtypeStruct(head_states.shape, F32)),
         in_specs=[pl.BlockSpec(memory_space=pl.ANY)] * len(args),
-        out_specs=(pl.BlockSpec(memory_space=pltpu.VMEM), pl.BlockSpec(memory_space=pl.ANY)),
+        out_specs=(pl.BlockSpec(memory_space=pltpu.VMEM), pl.BlockSpec(memory_space=pltpu.VMEM)),
         scratch_shapes=scratch,
-        compiler_params=pltpu.CompilerParams(collective_id=0, has_side_effects=True, vmem_limit_bytes=56 * 1024 * 1024),
+        compiler_params=pltpu.CompilerParams(collective_id=0, has_side_effects=True, vmem_limit_bytes=40 * 1024 * 1024),
     )(*args)
+
+    def tail(lo_ref, ns_ref, o_ref, on_ref, sem):
+        cps = [pltpu.make_async_copy(lo_ref, o_ref, sem.at[8])]
+        for i in range(8):
+            at = (i // 4, pl.ds(128 * (i % 4), 128))
+            cps.append(pltpu.make_async_copy(ns_ref.at[at], on_ref.at[at], sem.at[i]))
+        for cp in cps:
+            cp.start()
+        for cp in cps:
+            cp.wait()
+
+    return pl.pallas_call(
+        tail,
+        out_shape=(jax.ShapeDtypeStruct(residual.shape, BF16), jax.ShapeDtypeStruct(head_states.shape, F32)),
+        in_specs=[pl.BlockSpec(memory_space=pltpu.VMEM), pl.BlockSpec(memory_space=pltpu.VMEM)],
+        out_specs=(pl.BlockSpec(memory_space=pl.ANY), pl.BlockSpec(memory_space=pl.ANY)),
+        scratch_shapes=[pltpu.SemaphoreType.DMA((9,))],
+        compiler_params=pltpu.CompilerParams(vmem_limit_bytes=16 * 1024 * 1024),
+    )(lo, ns)
 
 
 def solution(mesh):

time: 65.1 us -> 59.8 us (0.919)
  local copies, waits for them, and re-layouts: 6.05 us -> 0 us
  Pallas kernels: 58.2 us -> 59.1 us
    unnamed x2 -> x0, local copies, waits for them, and re-layouts: 6.05 us -> none
    pallas_call x0 -> x1, Pallas kernels: none -> 2.08 us  [per_device(): pl.pallas_call(tail, out_shape=(jax.ShapeDtypeStruct(residual.shape, BF16...]
    pallas_call x1, Pallas kernels: 58.2 us -> 57 us  [per_device(): pl.pallas_call(functools.partial(kernel, N), out_shape=(jax.ShapeDtypeStr...]
where the time goes in v2:
time: 59.8 us; the launch traced here: 59.7 us
  Pallas kernels  59.1 us (99%)
  between operations  0.65 us (1%)
    pallas_call x1, Pallas kernels, per_device(): pl.pallas_call(functools.partial(kernel, N), out_shape=(jax.ShapeDtypeStr...  57 us
    pallas_call x1, Pallas kernels, per_device(): pl.pallas_call(tail, out_shape=(jax.ShapeDtypeStruct(residual.shape, BF16...  2.08 us

profile of v2, /device:TPU:69, one launch (start us, length us, event | category | flops | bytes accessed | tf_op | source)
XLA Modules:
  0.0 59.7 jit_solution(3317188792223642949)
XLA Ops:
  0.6 57.0 %shard_map.194 = (bf16[16,128]{1,0:T(8,128)(2,1)S(1)}, f32[2,512,1024]{2,1,0:T(8,128)S(1)}) custom-call(bf16[16,128]{1,0:T(8,128)(2,1)} %res_h.1, f32[2,512,1024]{2,1,0:T(8,128)} %st_h.1, bf16[32,128]{1,0:T(8,128)(2,1)} %bitcast.13, bf16[64,4096]{1,0:T(8,128)(2,1)} %bitcast.10, bf16[64,4096]{1,0:T(8,128)(2,1)} %bitcast.11, bf16[4096,128]{1,0:T(8,128)(2,1)} %wv_h.1, ...), custom_call_target="tpu_custom_call" | custom-call | tf_op jit(solution)/shard_map/pallas_call | solution.py:328
  57.6 2.1 %shard_map.195 = (bf16[16,128]{1,0:T(8,128)(2,1)}, f32[2,512,1024]{2,1,0:T(8,128)}) custom-call(bf16[16,128]{1,0:T(8,128)(2,1)S(1)} %get-tuple-element.4.lo_ref, f32[2,512,1024]{2,1,0:T(8,128)S(1)} %get-tuple-element.5.ns_ref), custom_call_target="tpu_custom_call" | custom-call | tf_op jit(solution)/shard_map/pallas_call | solution.py:347

commit v3 on v2

--- a/solution.py
+++ b/solution.py
@@ -29,7 +29,7 @@
     rt_h, gl_h, el_h, eg_h, eu_h, ed_h,
     out_ref, st,
     res, g1, wqk, wvg, wd, bias, hg, wo, g2, rt, gl, el, eg, eu, ed,
-    g1f, g2f, xb, pj, rq, decb, cols, mx, mb, ff, ch, sb, eb, db, rb, strm,
+    g1f, g2f, xb, pj, rq, decb, cols, mx, mb, ff, ch, cht, sb, eb, db, rb, rs, ps, pr,
     lsem, ssem, rsem, r1, r3, r4, osem,
 ):
     me = lax.axis_index("ep")
@@ -45,27 +45,48 @@
     barrier = pltpu.get_barrier_semaphore()
     reach = C // 4
     close = [o for o in near if abs(o) <= reach]
-    for o in close:
+    for o in close[::-1]:
         for cc in (0, 1):
             pl.semaphore_signal(barrier, inc=1, device_id={"ep": 2 * chip(o) + cc}, device_id_type=MESH)
     pl.semaphore_signal(barrier, inc=1, device_id={"ep": 2 * z + 1 - c}, device_id_type=MESH)
 
     half = pl.multiple_of(c * 1024, 1024)
     hrow = pl.multiple_of(c * 8, 8)
+    kmine, kother = pl.multiple_of(c * 2048, 2048), pl.multiple_of(2048 - c * 2048, 2048)
+    lmine, lother = pl.multiple_of(c * 128, 128), pl.multiple_of(128 - c * 128, 128)
     loads = [
         (res_h, res), (g1_h, g1), (g2_h, g2), (hg_h, hg), (rt_h, rt), (gl_h, gl), (el_h, el),
         (bias_h.at[pl.ds(hrow, 8)], bias), (wd_h.at[:, pl.ds(half, 1024)], wd),
         (wq_h, wqk.at[pl.ds(0, 64)]), (wk_h, wqk.at[pl.ds(64, 64)]), (wl_h, wqk.at[pl.ds(128, 16)]),
         (wv_h, wvg.at[:, pl.ds(0, 128)]), (wg_h, wvg.at[:, pl.ds(128, 128)]),
-        (st_h, st), (wo_h, wo), (eg_h.at[0], eg), (eu_h.at[0], eu), (ed_h.at[0], ed),
+        (st_h, st), (wo_h.at[pl.ds(kmine, 2048)], wo.at[:, pl.ds(lmine, 128)]), (eg_h.at[0], eg), (eu_h.at[0], eu), (ed_h.at[0], ed),
     ]
     cps = [pltpu.make_async_copy(s, d, lsem.at[i]) for i, (s, d) in enumerate(loads)]
     for cp in cps[:14]:
         cp.start()
-    for cp in cps[:9]:
+    cps[0].wait()
+
+    xb[me] = res[...]
+    pl.semaphore_wait(barrier, 2 * len(close) + 1)
+
+    def remote(src, dst, send, recv, j):
+        return pltpu.make_async_remote_copy(
+            src_ref=src, dst_ref=dst, send_sem=send, recv_sem=recv, device_id={"ep": j}, device_id_type=MESH
+        )
+
+
+    def arrived(buf, sem, o):
+        zz = chip(o)
+        ref = buf.at[pl.ds(2 * zz, 2)] if o else buf.at[2 * zz]
+        remote(ref, ref, sem.at[zz], sem.at[zz], me).wait_recv()
+        return zz
+
+    for o in close[::-1]:
+        for cc in (0, 1):
+            remote(res, xb.at[me], ssem.at[0], r1.at[z], 2 * chip(o) + cc).start()
+    remote(res, xb.at[me], ssem.at[0], r1.at[z], 2 * z + 1 - c).start()
+    for cp in cps[1:9]:
         cp.wait()
-
-    xb[me] = res[...]
     g1f[...] = g1[...].astype(F32)
     g2f[...] = g2[...].astype(F32)
 
@@ -91,32 +112,17 @@
     hit = jnp.where((r0 == expert) | (r1_ == expert), 1.0, 0.0)
     slot = mm(hit.astype(BF16), before)
     parity = (row - 2 * expert).astype(F32)
-    ch[...] = jnp.where(slot == parity, hit, 0.0)
+    chv = jnp.where(slot == parity, hit, 0.0)
+    ch[...] = chv.astype(BF16)
+    cht[...] = chv.T.astype(BF16)
     my_hit = jnp.where(routes == me, 1.0, 0.0)
     share = jnp.sum(weight * my_hit, axis=0, keepdims=True)
     mine = jnp.sum(my_hit, axis=0, keepdims=True)
     my_slot = mm(jnp.broadcast_to(mine, (8, T)).astype(BF16), before)
     srow = lax.broadcasted_iota(jnp.int32, (8, T), 0).astype(F32)
     rw = jnp.sum(jnp.where(my_slot == srow, jnp.broadcast_to(mine * share, (8, T)), 0.0), axis=1, keepdims=True)
-
-    pl.semaphore_wait(barrier, 2 * len(close) + 1)
-
-    def remote(src, dst, send, recv, j):
-        return pltpu.make_async_remote_copy(
-            src_ref=src, dst_ref=dst, send_sem=send, recv_sem=recv, device_id={"ep": j}, device_id_type=MESH
-        )
-
-
-    def arrived(buf, sem, o):
-        zz = chip(o)
-        ref = buf.at[pl.ds(2 * zz, 2)] if o else buf.at[2 * zz]
-        remote(ref, ref, sem.at[zz], sem.at[zz], me).wait_recv()
-        return zz
-
-    for o in close[::-1]:
-        for cc in (0, 1):
-            remote(res, xb.at[me], ssem.at[0], r1.at[z], 2 * chip(o) + cc).start()
-    remote(res, xb.at[me], ssem.at[0], r1.at[z], 2 * z + 1 - c).start()
+    my_rows = jnp.where(my_slot == srow, jnp.broadcast_to(mine, (8, T)), 0.0).astype(BF16)
+
     for o in close + [0]:
         zz = arrived(xb, r1, o)
         if 0 < o <= reach or -reach < o < 0:
@@ -163,6 +169,13 @@
     @pl.when(core == c)
     def _():
         rq[mine_at] = pj[z]
+
+    other = 2 * z + 1 - c
+    wsend = remote(wo_h.at[pl.ds(kother, 2048)], wo.at[:, pl.ds(lmine, 128)], ssem.at[5], rsem.at[3], other)
+    wsend.start()
+    for s in range(C):
+        both = jnp.concatenate([xb[2 * s], xb[2 * s + 1]], axis=1)
+        rs[s] = mm(my_rows, both)
 
     pick = jnp.where(lax.broadcasted_iota(jnp.int32, (T, 128), 0) == z, 1.0, 0.0)
     lowcol = mm(low, pick, TN, lax.Precision.HIGHEST)
@@ -213,10 +226,9 @@
         mixed.append(read * nrm * hg[...].astype(F32) * (g / (1.0 + jnp.exp(-g))))
     mixed = jnp.concatenate(mixed, axis=0).astype(BF16)
     mx[...] = mixed
-    mb[me] = mixed
+    mb[z] = mixed
     for o in far:
-        remote(mx, mb.at[me], ssem.at[2], r3.at[z], 2 * chip(o) + c).start()
-    remote(mx, mb.at[me], ssem.at[2], rsem.at[2], 2 * z + 1 - c).start()
+        remote(mx, mb.at[z], ssem.at[2], r3.at[z], 2 * chip(o) + c).start()
 
     for j in range(2):
         for i in range(8):
@@ -229,69 +241,73 @@
                     sl = (j, slice(r, r + 8), slice(128 * l, 128 * l + 128))
                     st[sl] = st[sl] * d8 + k8 * val[8 * j + l : 8 * j + l + 1]
     cps[15].wait()
+    wref = wo.at[:, pl.ds(lother, 128)]
+    remote(wref, wref, rsem.at[3], rsem.at[3], me).wait_recv()
     for o in near:
         zz = chip(o)
-        blk = mb.at[2 * zz + c]
+        blk = mb.at[zz]
         remote(blk, blk, r3.at[zz], r3.at[zz], me).wait_recv()
-        remote(blk, blk, ssem.at[2], rsem.at[2], 2 * z + 1 - c).start()
     PITCH = 17
     for s in range(T):
-        ff[c, s * PITCH : s * PITCH + 16] = mb[2 * s + c].astype(F32)
-    half_mb = mb.at[pl.ds(0, C)]
-    remote(half_mb, half_mb, rsem.at[2], rsem.at[2], me).wait_recv()
-    for s in range(T):
-        ff[1 - c, s * PITCH : s * PITCH + 16] = mb[2 * s + 1 - c].astype(F32)
+        ff[s * PITCH : s * PITCH + 16] = mb[s].astype(F32)
     lhs = []
-    for kb in range(N):
-        lhs.append(ff[kb // 16, pl.ds(kb % 16, T, stride=PITCH), :].astype(BF16))
-    branch = mm(jnp.concatenate(lhs, axis=1), wo[...]).astype(BF16).astype(F32)
-    stream = (res[...].astype(F32) + branch).astype(BF16)
-    strm[...] = stream
-
-    picked = mm(ch[...].astype(BF16), stream)
-    sb[...] = picked.reshape(N, 2, 128).astype(sb.dtype)
+    for kb in range(N // 2):
+        lhs.append(ff[pl.ds(kb, T, stride=PITCH), :].astype(BF16))
+    part = mm(jnp.concatenate(lhs, axis=1), wo[...]).astype(BF16)
+
+    sb[...] = mm(ch[...], part).reshape(N, 2, 256).astype(BF16)
     for o in far:
         for cc in (0, 1):
             j = 2 * chip(o) + cc
             remote(sb.at[j], eb.at[me], ssem.at[3], r4.at[z], j).start()
-    remote(sb.at[2 * z + 1 - c], eb.at[me], ssem.at[3], r4.at[z], 2 * z + 1 - c).start()
+    remote(sb.at[other], eb.at[me], ssem.at[3], r4.at[z], other).start()
     eb[me] = sb[me]
+    ps[0] = part[:, :128]
+    ps[1] = part[:, 128:]
+    remote(ps.at[1 - c], pr, ssem.at[6], rsem.at[2], other).start()
     for cp in cps[16:18]:
         cp.wait()
     ssq = jnp.zeros((2, 256), F32)
     ga = jnp.zeros((2, 512), F32)
     up = jnp.zeros((2, 512), F32)
-    for o in [0] + near:
-        zz = arrived(eb, r4, o)
-        x = jnp.concatenate([eb[2 * zz], eb[2 * zz + 1]], axis=1).astype(F32)
-        gain = jnp.concatenate([g2f[pl.ds(2 * zz, 1)], g2f[pl.ds(2 * zz + 1, 1)]], axis=1)
-        ssq = ssq + x * x
-        y = (x * gain).astype(BF16)
-        at = pl.multiple_of(zz * 256, 256)
-        ga = ga + mm(y, eg[pl.ds(at, 256), :])
-        up = up + mm(y, eu[pl.ds(at, 256), :])
+    pairs = [[0]] + [[d, -d] for d in range(1, C // 2)] + [[C // 2]]
+    for group in pairs:
+        zs = [arrived(eb, r4, o) for o in group]
+        for zz in zs:
+            branch = (eb[2 * zz].astype(F32) + eb[2 * zz + 1].astype(F32)).astype(BF16).astype(F32)
+            x = (rs[zz, 0:2] + branch).astype(BF16).astype(F32)
+            gain = jnp.concatenate([g2f[pl.ds(2 * zz, 1)], g2f[pl.ds(2 * zz + 1, 1)]], axis=1)
+            ssq = ssq + x * x
+            y = (x * gain).astype(BF16)
+            at = pl.multiple_of(zz * 256, 256)
+            ga = ga + mm(y, eg[pl.ds(at, 256), :])
+            up = up + mm(y, eu[pl.ds(at, 256), :])
     scale = lax.rsqrt(jnp.sum(ssq, axis=1, keepdims=True) * (1.0 / (128 * N)) + EPS)
     ga = ga * scale
     act = (ga / (1.0 + jnp.exp(-ga)) * (up * scale) * rw[0:2]).astype(BF16)
 
     cps[18].wait()
-    for o in far + [0]:
-        zz = chip(o)
-        at = pl.multiple_of(zz * 256, 256)
-        rows = mm(act, ed[:, pl.ds(at, 256)])
-        for cc in (0, 1):
-            db[2 * zz + cc] = rows[:, 128 * cc : 128 * cc + 128].astype(BF16).astype(db.dtype)
-            if o:
-                remote(db.at[2 * zz + cc], rb.at[me], ssem.at[4], rsem.at[1], 2 * zz + cc).start()
+    for group in pairs[::-1]:
+        zs = [chip(o) for o in group]
+        rows = [mm(act, ed[:, pl.ds(pl.multiple_of(zz * 256, 256), 256)]).astype(BF16) for zz in zs]
+        for zz, both in zip(zs, rows):
+            for cc in (0, 1):
+                db[2 * zz + cc] = both[:, 128 * cc : 128 * cc + 128]
+                if group[0]:
+                    remote(db.at[2 * zz + cc], rb.at[me], ssem.at[4], rsem.at[1], 2 * zz + cc).start()
     remote(db.at[2 * z + 1 - c], rb.at[me], ssem.at[4], rsem.at[1], 2 * z + 1 - c).start()
     rb[me] = db[me]
+    remote(pr, pr, rsem.at[2], rsem.at[2], me).wait_recv()
+    branch = (ps[c].astype(F32) + pr[...].astype(F32)).astype(BF16).astype(F32)
+    stream = (res[...].astype(F32) + branch).astype(BF16).astype(F32)
     ref = rb.at[pl.ds(0, N - 1)]
     remote(ref, ref, rsem.at[1], rsem.at[1], me).wait_recv()
-    back = mm(ch[...].astype(BF16), rb[...].reshape(2 * N, 128).astype(BF16), TN)
-    out_ref[...] = (strm[...].astype(F32) + back).astype(BF16)
-
-    for stage, ref in ((0, xb.at[pl.ds(0, N - 1)]), (2, mb.at[pl.ds(0, N - 1)]), (3, eb.at[pl.ds(0, N - 1)]), (4, rb.at[pl.ds(0, N - 1)])):
+    back = mm(cht[...], rb[...].reshape(2 * N, 128))
+    out_ref[...] = (stream + back).astype(BF16)
+
+    for stage, ref in ((0, xb.at[pl.ds(0, N - 1)]), (2, mb.at[pl.ds(0, C - 1)]), (6, pr), (3, eb.at[pl.ds(0, N - 1)]), (4, rb.at[pl.ds(0, N - 1)])):
         remote(ref, ref, ssem.at[stage], ssem.at[stage], me).wait_send()
+    wsend.wait_send()
 
     @pl.when(core == c)
     def _():
@@ -316,12 +332,12 @@
     SB = BF16
     scratch = [
         V((16, 128), BF16), V((N, 128), BF16), V((144, D), BF16), V((D, 256), BF16),
-        V((16, 1024), BF16), V((8, 128), F32), V((8, 128), BF16), V((D, 128), BF16), V((N, 128), BF16),
+        V((16, 1024), BF16), V((8, 128), F32), V((8, 128), BF16), V((D // 2, 256), BF16), V((N, 128), BF16),
         V((2, 16), jnp.int32), V((4, 16), F32), V((2, 16), F32), V((D, 512), BF16), V((D, 512), BF16), V((512, D), BF16),
         V((N, 128), F32), V((N, 128), F32), V((N, 16, 128), BF16), V((16, 4, 128), F32), V((16, 4, 128), F32),
-        V((1024, 128), F32), V((128, 128), F32), V((16, 128), BF16), V((N, 16, 128), BF16), V((2, 17 * 16, 128), F32),
-        V((2 * N, 16), F32), V((N, 2, 128), SB), V((N, 2, 128), SB), V((N, 2, 128), SB), V((N, 2, 128), SB), V((16, 128), BF16),
-        pltpu.SemaphoreType.DMA((19,)), pltpu.SemaphoreType.DMA((5,)), pltpu.SemaphoreType.DMA((3,)),
+        V((1024, 128), F32), V((128, 128), F32), V((16, 128), BF16), V((N // 2, 16, 128), BF16), V((17 * 16, 128), F32),
+        V((2 * N, 16), BF16), V((16, 2 * N), BF16), V((N, 2, 256), SB), V((N, 2, 256), SB), V((N, 2, 128), SB), V((N, 2, 128), SB), V((N // 2, 8, 256), F32), V((2, 16, 128), BF16), V((16, 128), BF16),
+        pltpu.SemaphoreType.DMA((19,)), pltpu.SemaphoreType.DMA((7,)), pltpu.SemaphoreType.DMA((4,)),
         pltpu.SemaphoreType.DMA((N // 2,)), pltpu.SemaphoreType.DMA((N // 2,)), pltpu.SemaphoreType.DMA((N // 2,)),
         pltpu.SemaphoreType.DMA((1,)),
     ]

time: 59.8 us -> 59 us (0.987)
  Pallas kernels: 59.1 us -> 58.3 us
    pallas_call x1, Pallas kernels: 57 us -> 56.2 us  [per_device(): pl.pallas_call(functools.partial(kernel, N), out_shape=(jax.ShapeDtypeStr...]
where the time goes in v3:
time: 59 us; the launch traced here: 58.9 us
  Pallas kernels  58.3 us (99%)
  between operations  0.65 us (1%)
    pallas_call x1, Pallas kernels, per_device(): pl.pallas_call(functools.partial(kernel, N), out_shape=(jax.ShapeDtypeStr...  56.2 us
    pallas_call x1, Pallas kernels, per_device(): pl.pallas_call(tail, out_shape=(jax.ShapeDtypeStruct(residual.shape, BF16...  2.08 us

profile of v3, /device:TPU:69, one launch (start us, length us, event | category | flops | bytes accessed | tf_op | source)
XLA Modules:
  0.0 58.9 jit_solution(15064459607729601508)
XLA Ops:
  0.6 56.2 %shard_map.194 = (bf16[16,128]{1,0:T(8,128)(2,1)S(1)}, f32[2,512,1024]{2,1,0:T(8,128)S(1)}) custom-call(bf16[16,128]{1,0:T(8,128)(2,1)} %res_h.1, f32[2,512,1024]{2,1,0:T(8,128)} %st_h.1, bf16[32,128]{1,0:T(8,128)(2,1)} %bitcast.13, bf16[64,4096]{1,0:T(8,128)(2,1)} %bitcast.10, bf16[64,4096]{1,0:T(8,128)(2,1)} %bitcast.11, bf16[4096,128]{1,0:T(8,128)(2,1)} %wv_h.1, ...), custom_call_target="tpu_custom_call" | custom-call | tf_op jit(solution)/shard_map/pallas_call | solution.py:344
  56.8 2.1 %shard_map.195 = (bf16[16,128]{1,0:T(8,128)(2,1)}, f32[2,512,1024]{2,1,0:T(8,128)}) custom-call(bf16[16,128]{1,0:T(8,128)(2,1)S(1)} %get-tuple-element.4.lo_ref, f32[2,512,1024]{2,1,0:T(8,128)S(1)} %get-tuple-element.5.ns_ref), custom_call_target="tpu_custom_call" | custom-call | tf_op jit(solution)/shard_map/pallas_call | solution.py:363

commit v4 on v3

--- a/solution.py
+++ b/solution.py
@@ -29,8 +29,8 @@
     rt_h, gl_h, el_h, eg_h, eu_h, ed_h,
     out_ref, st,
     res, g1, wqk, wvg, wd, bias, hg, wo, g2, rt, gl, el, eg, eu, ed,
-    g1f, g2f, xb, pj, rq, decb, cols, mx, mb, ff, ch, cht, sb, eb, db, rb, rs, ps, pr,
-    lsem, ssem, rsem, r1, r3, r4, osem,
+    g1f, g2f, xb, pj, rq, decb, mx, mb, ff, ch, cht, sb, eb, db, rb, rs, ps, pr,
+    lsem, ssem, rsem, r1, r3, r4, r2,
 ):
     me = lax.axis_index("ep")
     C = N // 2
@@ -160,11 +160,11 @@
     mine_at = lax.rem(me, S)
     for o in far:
         s = chip(o)
-        remote(pj.at[s], rq.at[mine_at], ssem.at[1], rsem.at[0], 2 * s + core).start()
+        remote(pj.at[s], rq.at[mine_at], ssem.at[1], r2.at[mine_at // 8], 2 * s + core).start()
 
     @pl.when(core != c)
     def _():
-        remote(pj.at[z], rq.at[mine_at], ssem.at[1], rsem.at[0], 2 * z + core).start()
+        remote(pj.at[z], rq.at[mine_at], ssem.at[1], r2.at[mine_at // 8], 2 * z + core).start()
 
     @pl.when(core == c)
     def _():
@@ -184,32 +184,35 @@
     for b in range(8):
         v = pre[b * 128 : (b + 1) * 128] + bcol[:, b : b + 1]
         ls = jnp.minimum(v, 0.0) - jnp.log(1.0 + jnp.exp(-jnp.abs(v)))
-        decb[b * 128 : (b + 1) * 128] = jnp.exp(ls * (1.0 / TAU))
+        decb[b // 4, (b % 4) * 128 : (b % 4 + 1) * 128] = jnp.exp(ls * (1.0 / TAU))
     cps[14].wait()
 
-    @pl.when(core == c)
-    def _():
-        ref = rq.at[pl.ds(0, S - 1)]
-        remote(ref, ref, rsem.at[0], rsem.at[0], me).wait_recv()
-
-    @pl.when(core != c)
-    def _():
-        remote(rq, rq, rsem.at[0], rsem.at[0], me).wait_recv()
-
-    allv = rq[...]
-    val = allv[:, 0, :]
-    gat = allv[:, 1, :]
-    ct = allv[:, 2, :].T
-    cols[:, 0:16] = ct
-    prod = ct[0:64] * ct[64:128]
-    dotqk = jnp.sum(prod, axis=0, keepdims=True)
-    lane = lax.broadcasted_iota(jnp.int32, (1, 16), 1)
     sub8 = lax.broadcasted_iota(jnp.int32, (8, 128), 0)
-    mixed = []
-    for j in range(2):
+    quarter = C // 4
+    first = lax.rem((lax.rem(z - c * (C // 2) + C, C) + quarter) // (2 * quarter), 2)
+    heads = []
+    for j in (first, 1 - first):
+        own = jnp.logical_and(core == c, mine_at // 8 == j)
+
+        @pl.when(own)
+        def _():
+            ref = rq.at[pl.ds(0, 7)]
+            remote(ref, ref, r2.at[j], r2.at[j], me).wait_recv()
+
+        @pl.when(jnp.logical_not(own))
+        def _():
+            ref = rq.at[pl.ds(0, 8)]
+            remote(ref, ref, r2.at[j], r2.at[j], me).wait_recv()
+
+        allv = rq[pl.ds(pl.multiple_of(8 * j, 8), 8)]
+        val = allv[:, 0, :]
+        g = allv[:, 1, :]
+        ct = allv[:, 2, :].T
+        heads.append((j, val, ct))
+        sqk = jnp.sum(jnp.sum(ct[0:64] * ct[64:128], axis=0, keepdims=True), axis=1, keepdims=True)
         acc = [jnp.zeros((8, 128), F32) for _ in range(8)]
         for i in range(8):
-            qd = jnp.broadcast_to(ct[0:64, 8 * j + i : 8 * j + i + 1], (64, 128)) * decb[j * 512 + i * 64 : j * 512 + (i + 1) * 64]
+            qd = jnp.broadcast_to(ct[0:64, i : i + 1], (64, 128)) * decb[j, i * 64 : (i + 1) * 64]
             for k in range(8):
                 q8 = qd[8 * k : 8 * k + 8]
                 r = i * 64 + 8 * k
@@ -218,28 +221,25 @@
         read = jnp.zeros((8, 128), F32)
         for l in range(8):
             read = jnp.where(sub8 == l, jnp.sum(acc[l], axis=0, keepdims=True), read)
-        sqk = jnp.sum(jnp.where((lane >= 8 * j) & (lane < 8 * j + 8), dotqk, 0.0), axis=1, keepdims=True)
-        read = (read + sqk * val[8 * j : 8 * j + 8]) * (512 ** -0.5)
+        read = (read + sqk * val) * (512 ** -0.5)
         tot = jnp.sum(jnp.sum(read * read, axis=1, keepdims=True), axis=0, keepdims=True)
         nrm = lax.rsqrt(tot * (1.0 / 1024) + EPS)
-        g = gat[8 * j : 8 * j + 8]
-        mixed.append(read * nrm * hg[...].astype(F32) * (g / (1.0 + jnp.exp(-g))))
-    mixed = jnp.concatenate(mixed, axis=0).astype(BF16)
-    mx[...] = mixed
-    mb[z] = mixed
+        mixed = (read * nrm * hg[...].astype(F32) * (g / (1.0 + jnp.exp(-g)))).astype(BF16)
+        mx[j] = mixed
+        mb[z, j] = mixed
     for o in far:
         remote(mx, mb.at[z], ssem.at[2], r3.at[z], 2 * chip(o) + c).start()
 
-    for j in range(2):
+    for j, val, ct in heads:
         for i in range(8):
-            kc = jnp.broadcast_to(ct[64:128, 8 * j + i : 8 * j + i + 1], (64, 128))
+            kc = jnp.broadcast_to(ct[64:128, i : i + 1], (64, 128))
             for k in range(8):
                 r = i * 64 + 8 * k
-                d8 = decb[j * 512 + r : j * 512 + r + 8]
+                d8 = decb[j, r : r + 8]
                 k8 = kc[8 * k : 8 * k + 8]
                 for l in range(8):
                     sl = (j, slice(r, r + 8), slice(128 * l, 128 * l + 128))
-                    st[sl] = st[sl] * d8 + k8 * val[8 * j + l : 8 * j + l + 1]
+                    st[sl] = st[sl] * d8 + k8 * val[l : l + 1]
     cps[15].wait()
     wref = wo.at[:, pl.ds(lother, 128)]
     remote(wref, wref, rsem.at[3], rsem.at[3], me).wait_recv()
@@ -249,7 +249,7 @@
         remote(blk, blk, r3.at[zz], r3.at[zz], me).wait_recv()
     PITCH = 17
     for s in range(T):
-        ff[s * PITCH : s * PITCH + 16] = mb[s].astype(F32)
+        ff[s * PITCH : s * PITCH + 16] = jnp.concatenate([mb[s, 0].astype(F32), mb[s, 1].astype(F32)], axis=0)
     lhs = []
     for kb in range(N // 2):
         lhs.append(ff[pl.ds(kb, T, stride=PITCH), :].astype(BF16))
@@ -335,11 +335,11 @@
         V((16, 1024), BF16), V((8, 128), F32), V((8, 128), BF16), V((D // 2, 256), BF16), V((N, 128), BF16),
         V((2, 16), jnp.int32), V((4, 16), F32), V((2, 16), F32), V((D, 512), BF16), V((D, 512), BF16), V((512, D), BF16),
         V((N, 128), F32), V((N, 128), F32), V((N, 16, 128), BF16), V((16, 4, 128), F32), V((16, 4, 128), F32),
-        V((1024, 128), F32), V((128, 128), F32), V((16, 128), BF16), V((N // 2, 16, 128), BF16), V((17 * 16, 128), F32),
+        V((2, 512, 128), F32), V((2, 8, 128), BF16), V((N // 2, 2, 8, 128), BF16), V((17 * 16, 128), F32),
         V((2 * N, 16), BF16), V((16, 2 * N), BF16), V((N, 2, 256), SB), V((N, 2, 256), SB), V((N, 2, 128), SB), V((N, 2, 128), SB), V((N // 2, 8, 256), F32), V((2, 16, 128), BF16), V((16, 128), BF16),
         pltpu.SemaphoreType.DMA((19,)), pltpu.SemaphoreType.DMA((7,)), pltpu.SemaphoreType.DMA((4,)),
         pltpu.SemaphoreType.DMA((N // 2,)), pltpu.SemaphoreType.DMA((N // 2,)), pltpu.SemaphoreType.DMA((N // 2,)),
-        pltpu.SemaphoreType.DMA((1,)),
+        pltpu.SemaphoreType.DMA((2,)),
     ]
     lo, ns = pl.pallas_call(
         functools.partial(kernel, N),

time: 59 us -> 58.8 us (level)
  no operation moved by 1% of the time
where the time goes in v4:
time: 58.8 us; the launch traced here: 58.7 us
  Pallas kernels  58.1 us (99%)
  between operations  0.65 us (1%)
    pallas_call x1, Pallas kernels, per_device(): pl.pallas_call(functools.partial(kernel, N), out_shape=(jax.ShapeDtypeStr...  56 us
    pallas_call x1, Pallas kernels, per_device(): pl.pallas_call(tail, out_shape=(jax.ShapeDtypeStruct(residual.shape, BF16...  2.08 us

profile of v4, /device:TPU:69, one launch (start us, length us, event | category | flops | bytes accessed | tf_op | source)
XLA Modules:
  0.0 58.7 jit_solution(7931596023439014986)
XLA Ops:
  0.6 56.0 %shard_map.194 = (bf16[16,128]{1,0:T(8,128)(2,1)S(1)}, f32[2,512,1024]{2,1,0:T(8,128)S(1)}) custom-call(bf16[16,128]{1,0:T(8,128)(2,1)} %res_h.1, f32[2,512,1024]{2,1,0:T(8,128)} %st_h.1, bf16[32,128]{1,0:T(8,128)(2,1)} %bitcast.13, bf16[64,4096]{1,0:T(8,128)(2,1)} %bitcast.10, bf16[64,4096]{1,0:T(8,128)(2,1)} %bitcast.11, bf16[4096,128]{1,0:T(8,128)(2,1)} %wv_h.1, ...), custom_call_target="tpu_custom_call" | custom-call | tf_op jit(solution)/shard_map/pallas_call | solution.py:344
  56.6 2.1 %shard_map.195 = (bf16[16,128]{1,0:T(8,128)(2,1)}, f32[2,512,1024]{2,1,0:T(8,128)}) custom-call(bf16[16,128]{1,0:T(8,128)(2,1)S(1)} %get-tuple-element.4.lo_ref, f32[2,512,1024]{2,1,0:T(8,128)S(1)} %get-tuple-element.5.ns_ref), custom_call_target="tpu_custom_call" | custom-call | tf_op jit(solution)/shard_map/pallas_call | solution.py:363
